TPU v7x, 32 devices: a whole 2x2x4 slice. The times are simulated.
32 devices in a mesh: fs: 8 (over z, y), tp: 4 (over x, core).
Axes of the slice: x: 2, y: 2, z: 4, core: 2. Of those that a mesh axis runs over, the one named last changes fastest.
Arguments:
- inputs: bfloat16 [9216, 2048], P('fs'), may hold values from -6 to 6
- gate_cot: bfloat16 [9216, 4096], P('fs', 'tp'), may hold values from -0.0546875 to 0.0546875
- state_cot: bfloat16 [9216, 1024], P('fs', 'tp'), may hold values from -0.0546875 to 0.0546875
- gate_weight: float32 [2048, 4096], P('fs', 'tp'), may hold values from -0.75 to 0.75
- state_weight: float32 [2048, 1024], P('fs', 'tp'), may hold values from -0.75 to 0.75
- gate_factor: bfloat16 [2048, 256], P('fs'), may hold values from -0.375 to 0.375
- state_factor: bfloat16 [2048, 256], P('fs'), may hold values from -0.375 to 0.375
- gate_first: float32 [256, 4096], P('fs', 'tp'), may hold values from -6 to 6
- gate_second: float32 [256, 4096], P('fs', 'tp'), may hold values from 0.3 to 3
- state_first: float32 [256, 1024], P('fs', 'tp'), may hold values from -6 to 6
- state_second: float32 [256, 1024], P('fs', 'tp'), may hold values from 0.3 to 3
Outputs:
- new_gate_weight: float32 [2048, 4096], P('fs', 'tp')
- new_state_weight: float32 [2048, 1024], P('fs', 'tp')
- gate_copy: bfloat16 [2048, 4096], P(None, 'tp')
- state_copy: bfloat16 [2048, 1024], P(None, 'tp')
- new_gate_first: float32 [256, 4096], P('fs', 'tp')
- new_gate_second: float32 [256, 4096], P('fs', 'tp')
- new_state_first: float32 [256, 1024], P('fs', 'tp')
- new_state_second: float32 [256, 1024], P('fs', 'tp')
All inputs are finite; a program needn't handle non-finite values.
Results may differ from a plain program's by a relative error of at most 0.004.
Values may be sent and summed in bfloat16 or wider, within the bound.
No kernel may reach another device: no remote copies, remote signals or barrier semaphores. Data moves between devices by JAX's collectives and lax.ppermute only.
A program may use at most 128 MiB of HBM per device.

v0:
```python
import jax
import jax.numpy as jnp
from jax import lax
from jax.sharding import PartitionSpec as P

D = 2048
DI = 4096
BW = 1024


def lifted_product(inputs, factor, cot):
    lifted = jnp.dot(inputs, factor, preferred_element_type=jnp.float32)
    upper = lifted.astype(jnp.bfloat16)
    lower = (lifted - upper.astype(jnp.float32)).astype(jnp.bfloat16)
    first_part = jnp.einsum("tr,tc->rc", upper, cot, preferred_element_type=jnp.float32)
    return first_part + jnp.einsum("tr,tc->rc", lower, cot, preferred_element_type=jnp.float32)


def per_device(
    inputs,
    gate_cot,
    state_cot,
    gate_weight,
    state_weight,
    gate_factor,
    state_factor,
    gate_first,
    gate_second,
    state_first,
    state_second,
):
    gate_cols = gate_cot.shape[1]
    whole_gate, whole_state = (
        lax.all_gather(gate_factor, "fs", axis=0, tiled=True),
        lax.all_gather(state_factor, "fs", axis=0, tiled=True),
    )
    gate_part = lifted_product(inputs, whole_gate, gate_cot)
    state_part = lifted_product(inputs, whole_state, state_cot)
    partial_proj = jnp.concatenate([gate_part, state_part], 1)
    projection = lax.psum_scatter(partial_proj, "fs", scatter_dimension=0, tiled=True)
    first_old = jnp.concatenate([gate_first, state_first], 1)
    second_old = jnp.concatenate([gate_second, state_second], 1)
    first_new = 0.8 * first_old + 0.2 * projection
    second_new = 0.9 * second_old + 0.1 * projection * projection
    direction = (first_new / jnp.sqrt(second_new)).astype(jnp.bfloat16)
    all_dirs = lax.all_gather(direction, "fs", axis=0, tiled=True)
    gate_full = jnp.dot(gate_factor, all_dirs[:, :gate_cols], preferred_element_type=jnp.float32)
    state_full = jnp.dot(state_factor, all_dirs[:, gate_cols:], preferred_element_type=jnp.float32)
    gate_sq, state_sq = lax.psum(
        (jnp.sum(gate_full * gate_full), jnp.sum(state_full * state_full)), ("fs", "tp")
    )
    gate_scale = 0.02 / jnp.sqrt(gate_sq / (D * DI) + 0.25)
    state_scale = 0.02 / jnp.sqrt(state_sq / (D * BW) + 0.25)
    gate_new = gate_weight - gate_scale * gate_full
    state_new = state_weight - state_scale * state_full
    gate_copy, state_copy = (
        lax.all_gather(gate_new.astype(jnp.bfloat16), "fs", axis=0, tiled=True),
        lax.all_gather(state_new.astype(jnp.bfloat16), "fs", axis=0, tiled=True),
    )
    return (
        gate_new,
        state_new,
        gate_copy,
        state_copy,
        first_new[:, :gate_cols],
        second_new[:, :gate_cols],
        first_new[:, gate_cols:],
        second_new[:, gate_cols:],
    )


def solution(mesh):
    return jax.shard_map(
        per_device,
        mesh=mesh,
        in_specs=(
            P("fs", None),
            P("fs", "tp"),
            P("fs", "tp"),
            P("fs", "tp"),
            P("fs", "tp"),
            P("fs", None),
            P("fs", None),
            P("fs", "tp"),
            P("fs", "tp"),
            P("fs", "tp"),
            P("fs", "tp"),
        ),
        out_specs=(
            P("fs", "tp"),
            P("fs", "tp"),
            P(None, "tp"),
            P(None, "tp"),
            P("fs", "tp"),
            P("fs", "tp"),
            P("fs", "tp"),
            P("fs", "tp"),
        ),
        check_vma=False,
    )
```

profile of v0, /device:TPU:0, one launch (start us, length us, event | category | flops | bytes accessed | tf_op | source)
XLA Modules:
  0.0 370.5 jit_solution(9867147324126327805)
XLA Ops:
  8.7 44.4 %all-gather.5.cloned.1.call-done = bf16[2048,256]{1,0:T(8,128)(2,1)} async-done(((bf16[256,256]{1,0:T(8,128)(2,1)}), bf16[2048,256]{1,0:T(8,128)(2,1)}) %all-gather.5.cloned.1.call-update) | async-done | bytes 1048592 | tf_op jit(solution)/shard_map/all_gather | solution.py:34
  53.2 4.1 %fusion.16 = f32[1152,256]{1,0:T(8,128)S(1)} fusion(bf16[1152,2048]{1,0:T(8,128)(2,1)} %param.11, bf16[2048,256]{1,0:T(8,128)(2,1)} %all-gather.5.cloned.1.call-done), kind=kOutput, calls=%fused_computation.27 | convolution fusion | flops 1207959552 | bytes 6946816 | tf_op jit(solution)/shard_map/dot_general | solution.py:12
  59.0 35.3 %all-gather.7.cloned.1.call-done = bf16[2048,256]{1,0:T(8,128)(2,1)} async-done(((bf16[256,256]{1,0:T(8,128)(2,1)}), bf16[2048,256]{1,0:T(8,128)(2,1)}) %all-gather.7.cloned.1.call-update) | async-done | bytes 1048592 | tf_op jit(solution)/shard_map/all_gather | solution.py:35
  94.3 4.1 %fusion.17 = f32[1152,256]{1,0:T(8,128)S(1)} fusion(bf16[1152,2048]{1,0:T(8,128)(2,1)} %param.11, bf16[2048,256]{1,0:T(8,128)(2,1)} %all-gather.7.cloned.1.call-done), kind=kOutput, calls=%fused_computation.28 | convolution fusion | flops 1207959552 | bytes 6946816 | tf_op jit(solution)/shard_map/dot_general | solution.py:12
  99.2 1.2 pad_maximum_fusion
  102.1 62.2 %reduce-scatter.2.cloned.1.call-done = f32[32,1280]{1,0:T(8,128)} async-done(((f32[256,1280]{1,0:T(8,128)}), f32[32,1280]{1,0:T(8,128)}) %reduce-scatter.2.cloned.1.call-update) | async-done | bytes 163856 | tf_op jit(solution)/shard_map/reduce_scatter | solution.py:40
  164.4 1.7 multiply_convert_fusion
  166.1 32.1 %all_gather.17 = bf16[256,1280]{1,0:T(8,128)(2,1)S(1)} all-gather(bf16[32,1280]{1,0:T(8,128)(2,1)S(1)} %get-tuple-element.22), channel_id=1, replica_groups=mesh['fs'=8,'tp'=4] {'fs'}, dimensions={0}, use_global_device_ids=true | all-gather | bytes 737280 | tf_op jit(solution)/shard_map/all_gather | solution.py:46
  198.2 1.1 multiply_reduce_fusion
  199.2 1.5 multiply_reduce_fusion.1
  200.8 37.5 %all-reduce = (f32[]{:T(128)}, f32[]{:T(128)}) all-reduce(f32[]{:T(128)} %get-tuple-element.25, f32[]{:T(128)} %get-tuple-element.27), channel_id=1, replica_groups=mesh['fs'=8,'tp'=4] {'fs','tp'}, use_global_device_ids=true, to_apply=%region_2.0 | all-reduce | flops 2 | bytes 16 | tf_op jit(solution)/shard_map/psum | solution.py:49
  238.9 1.8 fusion.12
  240.8 2.5 copy.21
  244.0 2.5 fusion.13
  246.6 1.7 slice.26
  248.2 1.4 slice.28
  249.6 1.6 slice.27
  251.2 1.4 slice.29
  252.6 1.8 copy.24
  254.4 1.3 copy.23
  255.7 25.7 %all-gather.11.cloned.1.call-done = bf16[2048,256]{0,1:T(8,128)(2,1)} async-done(((bf16[256,256]{0,1:T(8,128)(2,1)}), bf16[2048,256]{0,1:T(8,128)(2,1)}) %all-gather.11.cloned.1.call-update) | async-done | bytes 1048592 | tf_op jit(solution)/shard_map/all_gather | solution.py:58
  281.4 2.3 copy.26
  283.7 73.9 %all-gather.9.cloned.1.call-done = bf16[2048,1024]{0,1:T(8,128)(2,1)} async-done(((bf16[256,1024]{0,1:T(8,128)(2,1)}), bf16[2048,1024]{0,1:T(8,128)(2,1)}) %all-gather.9.cloned.1.call-update) | async-done | bytes 4194320 | tf_op jit(solution)/shard_map/all_gather | solution.py:57
  357.5 6.4 %copy.25 = bf16[2048,1024]{1,0:T(8,128)(2,1)} copy(bf16[2048,1024]{0,1:T(8,128)(2,1)} %all-gather.9.cloned.1.call-done) | data formatting | bytes 8388608
  (35 shorter events, 5.9 us)
Async XLA Ops:
  7.2 50.0 %copy-start = (bf16[1152,1024]{1,0:T(8,128)(2,1)S(1)}, bf16[1152,1024]{1,0:T(8,128)(2,1)}, u32[]{:S(2)}) copy-start(bf16[1152,1024]{1,0:T(8,128)(2,1)} %param.12) | copy-start | bytes 7077892
  7.2 46.0 %all-gather.5.cloned.1.call-start = ((), (), s32[]{:S(2)}) async-start(), calls=%async_computation.1 | async-start | bytes 1179648 | tf_op jit(solution)/shard_map/all_gather | solution.py:34
  7.9 86.4 %all-gather.7.cloned.1.call-start = ((), (), s32[]{:S(2)}) async-start(), calls=%async_computation.2 | async-start | bytes 1179648 | tf_op jit(solution)/shard_map/all_gather | solution.py:35
  8.7 155.7 %reduce-scatter.2.cloned.1.call-start = ((), (), s32[]{:S(2)}) async-start(), calls=%async_computation.3 | async-start | bytes 1474560 | tf_op jit(solution)/shard_map/reduce_scatter | solution.py:40
  94.3 4.1 %copy-start.2 = (bf16[1152,256]{1,0:T(8,128)(2,1)S(1)}, bf16[1152,256]{1,0:T(8,128)(2,1)}, u32[]{:S(2)}) copy-start(bf16[1152,256]{1,0:T(8,128)(2,1)} %param.13) | copy-start | bytes 1769476
  100.3 0.9 copy-start.5
  100.3 64.0 %copy-start.6 = (f32[32,1024]{1,0:T(8,128)S(1)}, f32[32,1024]{1,0:T(8,128)}, u32[]{:S(2)}) copy-start(f32[32,1024]{1,0:T(8,128)} %param.19) | copy-start | bytes 393220
  100.3 64.0 %copy-start.7 = (f32[32,1024]{1,0:T(8,128)S(1)}, f32[32,1024]{1,0:T(8,128)}, u32[]{:S(2)}) copy-start(f32[32,1024]{1,0:T(8,128)} %param.18) | copy-start | bytes 393220
  100.3 64.0 %copy-start.8 = (f32[32,256]{1,0:T(8,128)S(1)}, f32[32,256]{1,0:T(8,128)}, u32[]{:S(2)}) copy-start(f32[32,256]{1,0:T(8,128)} %param.21) | copy-start | bytes 98308
  100.3 64.0 %copy-start.9 = (f32[32,256]{1,0:T(8,128)S(1)}, f32[32,256]{1,0:T(8,128)}, u32[]{:S(2)}) copy-start(f32[32,256]{1,0:T(8,128)} %param.20) | copy-start | bytes 98308
  100.4 97.8 %copy-start.3 = (bf16[256,256]{1,0:T(8,128)(2,1)S(1)}, bf16[256,256]{1,0:T(8,128)(2,1)}, u32[]{:S(2)}) copy-start(bf16[256,256]{1,0:T(8,128)(2,1)} %param.16) | copy-start | bytes 393220
  100.4 181.0 %all-gather.11.cloned.1.call-start = ((), (), s32[]{:S(2)}) async-start(), calls=%async_computation.5 | async-start | bytes 1179648 | tf_op jit(solution)/shard_map/all_gather | solution.py:58
  166.1 33.2 %copy-start.4 = (bf16[256,256]{1,0:T(8,128)(2,1)S(1)}, bf16[256,256]{1,0:T(8,128)(2,1)}, u32[]{:S(2)}) copy-start(bf16[256,256]{1,0:T(8,128)(2,1)} %param.17) | copy-start | bytes 393220
  240.8 116.8 %all-gather.9.cloned.1.call-start = ((), (), s32[]{:S(2)}) async-start(), calls=%async_computation.4 | async-start | bytes 4718592 | tf_op jit(solution)/shard_map/all_gather | solution.py:57
  246.6 7.8 %copy-start.1 = (f32[256,1024]{0,1:T(8,128)S(1)}, f32[256,1024]{0,1:T(8,128)}, u32[]{:S(2)}) copy-start(f32[256,1024]{0,1:T(8,128)} %get-tuple-element.21) | copy-start | bytes 3145732
Sparse Core Ops, SparseCore 0:
  10.1 42.9 all-gather.4
  55.3 38.9 all-gather.6
  100.5 63.7 reduce-scatter.1
  240.9 40.4 all-gather.10
  283.9 73.6 all-gather.8
where the time goes:
time: 371 us; the launch traced here: 370 us
  waiting for transfers between devices  243 us (65%)
  blocking collectives  69.6 us (19%)
  local copies, waits for them, and re-layouts  22 us (6%)
  between operations  15.3 us (4%)
  matrix products  13.3 us (4%)
  other arithmetic  7.18 us (2%)
    all_gather x1, waiting for transfers between devices, per_device(): lax.all_gather(gate_new.astype(jnp.bfloat16), 'fs', axis=0, tiled=True)  73.9 us
    reduce_scatter x1, waiting for transfers between devices, per_device(): lax.psum_scatter(partial_proj, 'fs', scatter_dimension=0, tiled=True)  62.2 us
    all_gather x1, waiting for transfers between devices, per_device(): lax.all_gather(gate_factor, 'fs', axis=0, tiled=True)  44.4 us
    psum x1, blocking collectives, per_device(): lax.psum((jnp.sum(gate_full * gate_full), jnp.sum(state_full * state_full...  37.5 us
    all_gather x1, waiting for transfers between devices, per_device(): lax.all_gather(state_factor, 'fs', axis=0, tiled=True)  35.3 us
    all_gather x1, blocking collectives, per_device(): all_dirs = lax.all_gather(direction, 'fs', axis=0, tiled=True)  32.1 us
    all_gather x1, waiting for transfers between devices, per_device(): lax.all_gather(state_new.astype(jnp.bfloat16), 'fs', axis=0, tiled=True)  25.7 us
    unnamed x26, local copies, waits for them, and re-layouts  16 us
  transfers between devices with their start and end apart: 5, of which 5 were waited for; matrix products, arithmetic and copies ran while one was open for 6% of the time, Pallas kernels for 0%

commit v1 on v0

--- a/solution.py
+++ b/solution.py
@@ -47,7 +47,7 @@
     gate_full = jnp.dot(gate_factor, all_dirs[:, :gate_cols], preferred_element_type=jnp.float32)
     state_full = jnp.dot(state_factor, all_dirs[:, gate_cols:], preferred_element_type=jnp.float32)
     gate_sq, state_sq = lax.psum(
-        (jnp.sum(gate_full * gate_full), jnp.sum(state_full * state_full)), ("fs", "tp")
+        lax.psum((jnp.sum(gate_full * gate_full), jnp.sum(state_full * state_full)), "tp"), "fs"
     )
     gate_scale = 0.02 / jnp.sqrt(gate_sq / (D * DI) + 0.25)
     state_scale = 0.02 / jnp.sqrt(state_sq / (D * BW) + 0.25)

time: 371 us -> 356 us (0.960)
  blocking collectives: 69.6 us -> 57.9 us
  waiting for transfers between devices: 243 us -> 239 us
    psum x1, blocking collectives: 37.5 us -> 6.27 us  [per_device(): lax.psum((jnp.sum(gate_full * gate_full), jnp.sum(state_full * state_full...]
    psum x0 -> x1, blocking collectives: none -> 19.6 us  [per_device(): lax.psum(lax.psum((jnp.sum(gate_full * gate_full), jnp.sum(state_full * s...]
where the time goes in v1:
time: 356 us; the launch traced here: 355 us
  waiting for transfers between devices  239 us (67%)
  blocking collectives  57.9 us (16%)
  local copies, waits for them, and re-layouts  22 us (6%)
  between operations  15.3 us (4%)
  matrix products  13.3 us (4%)
  other arithmetic  7.2 us (2%)
    all_gather x1, waiting for transfers between devices, per_device(): lax.all_gather(gate_new.astype(jnp.bfloat16), 'fs', axis=0, tiled=True)  73.9 us
    reduce_scatter x1, waiting for transfers between devices, per_device(): lax.psum_scatter(partial_proj, 'fs', scatter_dimension=0, tiled=True)  62.2 us
    all_gather x1, waiting for transfers between devices, per_device(): lax.all_gather(gate_factor, 'fs', axis=0, tiled=True)  44.4 us
    all_gather x1, waiting for transfers between devices, per_device(): lax.all_gather(state_factor, 'fs', axis=0, tiled=True)  35.3 us
    all_gather x1, blocking collectives, per_device(): all_dirs = lax.all_gather(direction, 'fs', axis=0, tiled=True)  32.1 us
    all_gather x1, waiting for transfers between devices, per_device(): lax.all_gather(state_new.astype(jnp.bfloat16), 'fs', axis=0, tiled=True)  22.2 us
    psum x1, blocking collectives, per_device(): lax.psum(lax.psum((jnp.sum(gate_full * gate_full), jnp.sum(state_full * s...  19.6 us
    unnamed x26, local copies, waits for them, and re-layouts  16 us
  transfers between devices with their start and end apart: 5, of which 5 were waited for; matrix products, arithmetic and copies ran while one was open for 6% of the time, Pallas kernels for 0%

profile of v1, /device:TPU:0, one launch (start us, length us, event | category | flops | bytes accessed | tf_op | source)
XLA Modules:
  0.0 355.3 jit_solution(6174143175390339941)
XLA Ops:
  8.7 44.4 %all-gather.5.cloned.1.call-done = bf16[2048,256]{1,0:T(8,128)(2,1)} async-done(((bf16[256,256]{1,0:T(8,128)(2,1)}), bf16[2048,256]{1,0:T(8,128)(2,1)}) %all-gather.5.cloned.1.call-update) | async-done | bytes 1048592 | tf_op jit(solution)/shard_map/all_gather | solution.py:34
  53.2 4.1 %fusion.16 = f32[1152,256]{1,0:T(8,128)S(1)} fusion(bf16[1152,2048]{1,0:T(8,128)(2,1)} %param.11, bf16[2048,256]{1,0:T(8,128)(2,1)} %all-gather.5.cloned.1.call-done), kind=kOutput, calls=%fused_computation.27 | convolution fusion | flops 1207959552 | bytes 6946816 | tf_op jit(solution)/shard_map/dot_general | solution.py:12
  59.0 35.3 %all-gather.7.cloned.1.call-done = bf16[2048,256]{1,0:T(8,128)(2,1)} async-done(((bf16[256,256]{1,0:T(8,128)(2,1)}), bf16[2048,256]{1,0:T(8,128)(2,1)}) %all-gather.7.cloned.1.call-update) | async-done | bytes 1048592 | tf_op jit(solution)/shard_map/all_gather | solution.py:35
  94.3 4.1 %fusion.17 = f32[1152,256]{1,0:T(8,128)S(1)} fusion(bf16[1152,2048]{1,0:T(8,128)(2,1)} %param.11, bf16[2048,256]{1,0:T(8,128)(2,1)} %all-gather.7.cloned.1.call-done), kind=kOutput, calls=%fused_computation.28 | convolution fusion | flops 1207959552 | bytes 6946816 | tf_op jit(solution)/shard_map/dot_general | solution.py:12
  99.2 1.2 pad_maximum_fusion
  102.1 62.2 %reduce-scatter.2.cloned.1.call-done = f32[32,1280]{1,0:T(8,128)} async-done(((f32[256,1280]{1,0:T(8,128)}), f32[32,1280]{1,0:T(8,128)}) %reduce-scatter.2.cloned.1.call-update) | async-done | bytes 163856 | tf_op jit(solution)/shard_map/reduce_scatter | solution.py:40
  164.4 1.7 multiply_convert_fusion
  166.1 32.1 %all_gather.17 = bf16[256,1280]{1,0:T(8,128)(2,1)S(1)} all-gather(bf16[32,1280]{1,0:T(8,128)(2,1)S(1)} %get-tuple-element.24), channel_id=1, replica_groups=mesh['fs'=8,'tp'=4] {'fs'}, dimensions={0}, use_global_device_ids=true | all-gather | bytes 737280 | tf_op jit(solution)/shard_map/all_gather | solution.py:46
  199.2 1.5 multiply_reduce_fusion.1
  200.8 6.3 %all-reduce.1 = (f32[]{:T(128)}, f32[]{:T(128)}) all-reduce(f32[]{:T(128)} %get-tuple-element.27, f32[]{:T(128)} %get-tuple-element.29), channel_id=1, replica_groups=mesh['fs'=8,'tp'=4] {'tp'}, use_global_device_ids=true, to_apply=%region_2.0 | all-reduce | flops 2 | bytes 16 | tf_op jit(solution)/shard_map/psum | solution.py:50
  207.0 19.6 %all-reduce = (f32[]{:T(128)}, f32[]{:T(128)}) all-reduce(f32[]{:T(128)} %get-tuple-element.18, f32[]{:T(128)} %get-tuple-element.19), channel_id=1, replica_groups=mesh['fs'=8,'tp'=4] {'fs'}, use_global_device_ids=true, to_apply=%region_3.0 | all-reduce | flops 2 | bytes 16 | tf_op jit(solution)/shard_map/psum | solution.py:49
  227.3 1.8 fusion.12
  229.2 2.5 copy.21
  232.4 2.5 fusion.13
  235.0 1.7 slice.26
  236.6 1.4 slice.28
  238.0 1.6 slice.27
  239.6 1.4 slice.29
  240.9 1.8 copy.24
  242.7 1.3 copy.23
  244.0 22.2 %all-gather.11.cloned.1.call-done = bf16[2048,256]{0,1:T(8,128)(2,1)} async-done(((bf16[256,256]{0,1:T(8,128)(2,1)}), bf16[2048,256]{0,1:T(8,128)(2,1)}) %all-gather.11.cloned.1.call-update) | async-done | bytes 1048592 | tf_op jit(solution)/shard_map/all_gather | solution.py:58
  266.2 2.3 copy.26
  268.4 73.9 %all-gather.9.cloned.1.call-done = bf16[2048,1024]{0,1:T(8,128)(2,1)} async-done(((bf16[256,1024]{0,1:T(8,128)(2,1)}), bf16[2048,1024]{0,1:T(8,128)(2,1)}) %all-gather.9.cloned.1.call-update) | async-done | bytes 4194320 | tf_op jit(solution)/shard_map/all_gather | solution.py:57
  342.3 6.4 %copy.25 = bf16[2048,1024]{1,0:T(8,128)(2,1)} copy(bf16[2048,1024]{0,1:T(8,128)(2,1)} %all-gather.9.cloned.1.call-done) | data formatting | bytes 8388608
  (36 shorter events, 7.0 us)
Async XLA Ops:
  7.2 50.0 %copy-start = (bf16[1152,1024]{1,0:T(8,128)(2,1)S(1)}, bf16[1152,1024]{1,0:T(8,128)(2,1)}, u32[]{:S(2)}) copy-start(bf16[1152,1024]{1,0:T(8,128)(2,1)} %param.12) | copy-start | bytes 7077892
  7.2 46.0 %all-gather.5.cloned.1.call-start = ((), (), s32[]{:S(2)}) async-start(), calls=%async_computation.1 | async-start | bytes 1179648 | tf_op jit(solution)/shard_map/all_gather | solution.py:34
  7.9 86.4 %all-gather.7.cloned.1.call-start = ((), (), s32[]{:S(2)}) async-start(), calls=%async_computation.2 | async-start | bytes 1179648 | tf_op jit(solution)/shard_map/all_gather | solution.py:35
  8.7 155.7 %reduce-scatter.2.cloned.1.call-start = ((), (), s32[]{:S(2)}) async-start(), calls=%async_computation.3 | async-start | bytes 1474560 | tf_op jit(solution)/shard_map/reduce_scatter | solution.py:40
  94.3 4.1 %copy-start.2 = (bf16[1152,256]{1,0:T(8,128)(2,1)S(1)}, bf16[1152,256]{1,0:T(8,128)(2,1)}, u32[]{:S(2)}) copy-start(bf16[1152,256]{1,0:T(8,128)(2,1)} %param.13) | copy-start | bytes 1769476
  100.3 0.9 copy-start.5
  100.3 64.0 %copy-start.6 = (f32[32,1024]{1,0:T(8,128)S(1)}, f32[32,1024]{1,0:T(8,128)}, u32[]{:S(2)}) copy-start(f32[32,1024]{1,0:T(8,128)} %param.19) | copy-start | bytes 393220
  100.3 64.0 %copy-start.7 = (f32[32,1024]{1,0:T(8,128)S(1)}, f32[32,1024]{1,0:T(8,128)}, u32[]{:S(2)}) copy-start(f32[32,1024]{1,0:T(8,128)} %param.18) | copy-start | bytes 393220
  100.3 64.0 %copy-start.8 = (f32[32,256]{1,0:T(8,128)S(1)}, f32[32,256]{1,0:T(8,128)}, u32[]{:S(2)}) copy-start(f32[32,256]{1,0:T(8,128)} %param.21) | copy-start | bytes 98308
  100.3 64.0 %copy-start.9 = (f32[32,256]{1,0:T(8,128)S(1)}, f32[32,256]{1,0:T(8,128)}, u32[]{:S(2)}) copy-start(f32[32,256]{1,0:T(8,128)} %param.20) | copy-start | bytes 98308
  100.4 97.8 %copy-start.3 = (bf16[256,256]{1,0:T(8,128)(2,1)S(1)}, bf16[256,256]{1,0:T(8,128)(2,1)}, u32[]{:S(2)}) copy-start(bf16[256,256]{1,0:T(8,128)(2,1)} %param.16) | copy-start | bytes 393220
  100.4 165.8 %all-gather.11.cloned.1.call-start = ((), (), s32[]{:S(2)}) async-start(), calls=%async_computation.5 | async-start | bytes 1179648 | tf_op jit(solution)/shard_map/all_gather | solution.py:58
  166.1 33.2 %copy-start.4 = (bf16[256,256]{1,0:T(8,128)(2,1)S(1)}, bf16[256,256]{1,0:T(8,128)(2,1)}, u32[]{:S(2)}) copy-start(bf16[256,256]{1,0:T(8,128)(2,1)} %param.17) | copy-start | bytes 393220
  229.1 113.2 %all-gather.9.cloned.1.call-start = ((), (), s32[]{:S(2)}) async-start(), calls=%async_computation.4 | async-start | bytes 4718592 | tf_op jit(solution)/shard_map/all_gather | solution.py:57
  234.9 7.8 %copy-start.1 = (f32[256,1024]{0,1:T(8,128)S(1)}, f32[256,1024]{0,1:T(8,128)}, u32[]{:S(2)}) copy-start(f32[256,1024]{0,1:T(8,128)} %get-tuple-element.23) | copy-start | bytes 3145732
Sparse Core Ops, SparseCore 0:
  10.1 42.9 all-gather.4
  55.3 38.9 all-gather.6
  100.5 63.7 reduce-scatter.1
  229.3 36.8 all-gather.10
  268.7 73.6 all-gather.8
